TPU v7x, 512 devices: a whole 4x4x16 slice. The times are simulated.
512 devices in a mesh: sp: 32 (over z, core), tp: 16 (over y, x).
Axes of the slice: x: 4, y: 4, z: 16, core: 2. Of those that a mesh axis runs over, the one named last changes fastest.
Arguments:
- resid: bfloat16 [6144, 2048], P('sp', 'tp'), may hold values from -12 to 12
- conv_value: bfloat16 [6144, 2048], P('sp', 'tp'), may hold values from -80 to 80
- conv_gate: bfloat16 [6144, 2048], P('sp', 'tp'), may hold values from -6 to 6
- depth_kernel: float32 [31, 2048], P(None, 'tp'), may hold values from -1 to 1
- chan_gain: float32 [2048], P('tp'), may hold values from 0.1 to 1.9
- point_weight: bfloat16 [2048, 2048], P('tp'), may hold values from -0.125 to 0.125
- mix_gain: float32 [2048], replicated, may hold values from 0.1 to 1.9
- out_weight: bfloat16 [2048, 2048], P(None, 'tp'), may hold values from -0.125 to 0.125
- norm_gain: float32 [2048], P('tp'), may hold values from 0.1 to 1.9
- route_ids: int32 [6144, 4], P('sp'), may hold values from 0 to 31, all different within a row; in each aligned block of 192 rows (0 to 191, 192 to 383, ...) at most 32 rows name the same one
- route_weights: float32 [6144, 4], P('sp'), may hold values from 0.05 to 0.5
- gate_experts: bfloat16 [32, 2048, 4096], P('sp', None, 'tp'), may hold values from -0.3125 to 0.3125
- up_experts: bfloat16 [32, 2048, 4096], P('sp', None, 'tp'), may hold values from -0.3125 to 0.3125
- down_experts: bfloat16 [32, 4096, 2048], P('sp', 'tp'), may hold values from -0.09375 to 0.09375
Outputs:
- result: bfloat16 [6144, 2048], P('sp', 'tp')
Inputs may be any that keep to these rules, and one draw needn't show every extreme that they name: `route_ids`: each row names 4 different experts; among the 192 rows of one index of sp no expert is named by more than 32 rows, and in some such block an expert is named by exactly 32.
All inputs are finite; a program needn't handle non-finite values.
Results may differ from a plain program's by a relative error of at most 0.024.
Values may be sent and summed in bfloat16 or wider, within the bound.
A program may use at most 64 MiB of HBM per device.

v0:
```python
import jax
import jax.numpy as jnp
from jax import lax
from jax.sharding import Mesh
from jax.sharding import PartitionSpec as P

E = 32
TOPK = 4
CAP = 32
TP = ("tp_0", "tp_1")
epsilon = 1e-05
clamp_limit = 7.0
swish_slope = 1.702


def from_behind(block, axis, distance):
    devices = range(lax.axis_size(axis))
    route = [(i - distance, i) for i in devices if i - distance in devices]
    return lax.ppermute(block, axis, route)


def over_axes(value, axes):
    for axis in axes:
        value = lax.psum(value, axis)
    return value


def split_up(value, dim, count):
    dims = value.shape
    pieces = value.reshape(*dims[:dim], count, dims[dim] // count, *dims[dim + 1 :])
    return jnp.moveaxis(pieces, dim, 0)


def summed_on_arrival(value, axis, dim):
    pieces = split_up(value, dim, lax.axis_size(axis))
    arrived = lax.all_to_all(pieces, axis, split_axis=0, concat_axis=0, tiled=True)
    return arrived.astype(jnp.float32).sum(axis=0)


def from_everyone(value, axis):
    copies = jnp.broadcast_to(value, (lax.axis_size(axis), *value.shape))
    return lax.all_to_all(copies, axis, split_axis=0, concat_axis=0, tiled=True)


def laid_out(pieces, dim):
    dims = list(pieces.shape[1:])
    dims[dim] *= pieces.shape[0]
    return jnp.moveaxis(pieces, 0, dim).reshape(dims)


def gathered_copies(value, axis, dim):
    pieces = from_everyone(value, axis)
    return laid_out(pieces, dim)


def shards(
    resid,
    conv_value,
    conv_gate,
    depth_kernel,
    chan_gain,
    point_weight,
    mix_gain,
    out_weight,
    norm_gain,
    route_ids,
    route_weights,
    gate_experts,
    up_experts,
    down_experts,
):
    tok_rows, chan_local = conv_value.shape
    feat_local = resid.shape[1]
    lookback = depth_kernel.shape[0] - 1
    gated = (conv_value.astype(jnp.float32) * jax.nn.sigmoid(conv_gate.astype(jnp.float32))).astype(
        jnp.bfloat16
    )
    earlier = from_behind(gated[tok_rows - lookback :], "sp", 1)
    padded = jnp.concatenate([earlier, gated], axis=0)
    conv = jnp.zeros((tok_rows, chan_local), jnp.float32)
    for tap in range(lookback + 1):
        conv = conv + padded[tap : tap + tok_rows].astype(jnp.float32) * depth_kernel[tap]
    chan_total = chan_local * lax.axis_size(TP)
    row_sums, row_squares = (
        over_axes(jnp.sum(conv, axis=1), TP),
        over_axes(jnp.sum(conv * conv, axis=1), TP),
    )
    row_mean = row_sums / chan_total
    row_var = row_squares / chan_total - row_mean * row_mean
    act = jax.nn.silu(
        (conv - row_mean[:, None]) * lax.rsqrt(row_var[:, None] + epsilon) * chan_gain
    ).astype(jnp.bfloat16)
    point = summed_on_arrival(
        jnp.dot(act, point_weight, preferred_element_type=jnp.float32).astype(jnp.bfloat16), TP, 0
    )
    mixed = (
        point * lax.rsqrt(jnp.mean(point * point, axis=1, keepdims=True) + epsilon) * mix_gain
    ).astype(jnp.bfloat16)
    branch = jnp.dot(gathered_copies(mixed, TP, 0), out_weight, preferred_element_type=jnp.float32)
    middle = (resid.astype(jnp.float32) + branch).astype(jnp.bfloat16)
    middle32 = middle.astype(jnp.float32)
    feat_total = feat_local * lax.axis_size(TP)
    squares = over_axes(jnp.sum(middle32 * middle32, axis=1), TP)
    normed = (middle32 * lax.rsqrt(squares[:, None] / feat_total + epsilon) * norm_gain).astype(
        jnp.bfloat16
    )
    flat_ids = route_ids.reshape(-1)
    expert_table = (flat_ids[:, None] == jnp.arange(E, dtype=jnp.int32)[None, :]).astype(jnp.int32)
    earlier_count = jnp.cumsum(expert_table, axis=0) - expert_table
    position = jnp.sum(earlier_count * expert_table, axis=1)
    slot_of = flat_ids * CAP + position
    slot_grid = slot_of.reshape(tok_rows, TOPK)
    picker = jnp.any(
        slot_grid[None, :, :] == jnp.arange(E * CAP, dtype=jnp.int32)[:, None, None], axis=2
    ).astype(jnp.bfloat16)
    outgoing = (
        jnp.dot(picker, normed, preferred_element_type=jnp.float32)
        .astype(jnp.bfloat16)
        .reshape(E, CAP, feat_local)
    )
    received = lax.all_gather(
        lax.all_to_all(outgoing, "sp", split_axis=0, concat_axis=0, tiled=True),
        TP,
        axis=2,
        tiled=True,
    )
    local_experts = gate_experts.shape[0]
    sources = received.shape[0] // local_experts
    count = received.shape[1]
    rows = received.reshape(sources, local_experts, count, received.shape[2])
    gate_pre = jnp.minimum(
        jnp.einsum("sjcd,jdf->sjcf", rows, gate_experts, preferred_element_type=jnp.float32),
        clamp_limit,
    )
    up_pre = jnp.clip(
        jnp.einsum("sjcd,jdf->sjcf", rows, up_experts, preferred_element_type=jnp.float32),
        -clamp_limit,
        clamp_limit,
    )
    hidden = (gate_pre * jax.nn.sigmoid(swish_slope * gate_pre) * (up_pre + 1.0)).astype(
        jnp.bfloat16
    )
    partial_value = jnp.einsum(
        "sjcf,jfd->sjcd", hidden, down_experts, preferred_element_type=jnp.float32
    )
    summed = summed_on_arrival(partial_value.astype(jnp.bfloat16), TP, 3).astype(jnp.bfloat16)
    returned = lax.all_to_all(
        summed.reshape(sources * local_experts, count, summed.shape[3]),
        "sp",
        split_axis=0,
        concat_axis=0,
        tiled=True,
    )
    flat_back = returned.reshape(E * CAP, feat_local)
    picked = flat_back[slot_of].astype(jnp.float32).reshape(tok_rows, TOPK, feat_local)
    routed_sum = jnp.sum(picked * route_weights[:, :, None], axis=1)
    return (middle32 + routed_sum).astype(jnp.bfloat16)


def solution(mesh):
    split = Mesh(mesh.devices.reshape(mesh.shape["sp"], 4, 4), ("sp", "tp_0", "tp_1"))
    return jax.shard_map(
        shards,
        mesh=split,
        in_specs=(
            P("sp", TP),
            P("sp", TP),
            P("sp", TP),
            P(None, TP),
            P(TP),
            P(TP, None),
            P(),
            P(None, TP),
            P(TP),
            P("sp", None),
            P("sp", None),
            P("sp", None, TP),
            P("sp", None, TP),
            P("sp", TP, None),
        ),
        out_specs=P("sp", TP),
        check_vma=False,
    )
```

profile of v0, /device:TPU:1, one launch (start us, length us, event | category | flops | bytes accessed | tf_op | source)
XLA Modules:
  0.0 313.9 jit_solution(2929535783332254951)
XLA Ops:
  7.5 4.9 %collective-permute-start = (bf16[30,128]{1,0:T(8,128)(2,1)S(1)}, bf16[30,128]{1,0:T(8,128)(2,1)S(1)}, u32[]{:S(2)}, u32[]{:S(2)}) collective-permute-start(bf16[30,128]{1,0:T(8,128)(2,1)S(1)} %slice.258), channel_id=1, source_target_pairs={{0,16},{16,32},{32,48},{48,64},{64,80},{80,96},{96,112},{112,128},... | collective-permute-start | bytes 23048 | tf_op jit(solution)/shard_map/ppermute | solution.py:19
  14.4 1.9 collective-permute-done
  16.8 7.1 %all-reduce.1 = (f32[192]{0:T(256)S(1)}, f32[192]{0:T(256)S(1)}) all-reduce(f32[192]{0:T(256)S(1)} %get-tuple-element.6, f32[192]{0:T(256)S(1)} %get-tuple-element.5), channel_id=1, replica_groups=mesh['sp'=32,'tp_0'=4,'tp_1'=4] {'tp_0'}, use_global_device_ids=true, to_apply=%region_4.0 | all-reduce | flops 384 | bytes 3072 | tf_op jit(solution)/shard_map/psum | solution.py:24
  23.9 8.2 %all-reduce = (f32[192]{0:T(256)S(1)}, f32[192]{0:T(256)S(1)}) all-reduce(f32[192]{0:T(256)S(1)} %get-tuple-element.9, f32[192]{0:T(256)S(1)} %get-tuple-element.10), channel_id=1, replica_groups=mesh['sp'=32,'tp_0'=4,'tp_1'=4] {'tp_1'}, use_global_device_ids=true, to_apply=%region_5.0 | all-reduce | flops 384 | bytes 3072 | tf_op jit(solution)/shard_map/psum | solution.py:24
  32.1 1.5 convolution_convert_fusion
  34.8 3.7 %all-to-all-start = ((bf16[16,12,2048]{2,1,0:T(8,128)(2,1)}), bf16[16,12,2048]{2,1,0:T(8,128)(2,1)S(1)}, u32[]{:S(2)}, u32[]{:S(2)}) async-start(bf16[16,12,2048]{2,1,0:T(8,128)(2,1)} %reshape.122), calls=%async_computation | async-start | bytes 2097152 | tf_op jit(solution)/shard_map/all_to_all | solution.py:36
  38.8 14.4 %all-to-all-done = bf16[16,12,2048]{2,1,0:T(8,128)(2,1)S(1)} async-done(((bf16[16,12,2048]{2,1,0:T(8,128)(2,1)}), bf16[16,12,2048]{2,1,0:T(8,128)(2,1)S(1)}, u32[]{:S(2)}, u32[]{:S(2)}) %all-to-all-start) | async-done | bytes 786464 | tf_op jit(solution)/shard_map/all_to_all | solution.py:36
  54.7 3.7 %all-to-all-start.1 = ((bf16[16,12,2048]{2,1,0:T(8,128)(2,1)}), bf16[16,12,2048]{2,1,0:T(8,128)(2,1)S(1)}, u32[]{:S(2)}, u32[]{:S(2)}) async-start(bf16[16,12,2048]{2,1,0:T(8,128)(2,1)} %broadcast_in_dim.2), calls=%async_computation.1 | async-start | bytes 2097152 | tf_op jit(solution)/shard_map/all_to_all | solution.py:42
  58.5 1.7 reduce-window.6
  61.5 1.2 fusion
  62.7 9.5 %all-to-all-done.1 = bf16[16,12,2048]{2,1,0:T(8,128)(2,1)S(1)} async-done(((bf16[16,12,2048]{2,1,0:T(8,128)(2,1)}), bf16[16,12,2048]{2,1,0:T(8,128)(2,1)S(1)}, u32[]{:S(2)}, u32[]{:S(2)}) %all-to-all-start.1) | async-done | bytes 786464 | tf_op jit(solution)/shard_map/all_to_all | solution.py:42
  72.8 7.3 %psum.46 = f32[192]{0:T(256)S(1)} all-reduce(f32[192]{0:T(256)S(1)} %get-tuple-element.47), channel_id=1, replica_groups=mesh['sp'=32,'tp_0'=4,'tp_1'=4] {'tp_0'}, use_global_device_ids=true, to_apply=%region_13.14 | all-reduce | flops 192 | bytes 1536 | tf_op jit(solution)/shard_map/psum | solution.py:24
  80.1 6.6 %psum.47 = f32[192]{0:T(256)S(1)} all-reduce(f32[192]{0:T(256)S(1)} %psum.46), channel_id=1, replica_groups=mesh['sp'=32,'tp_0'=4,'tp_1'=4] {'tp_1'}, use_global_device_ids=true, to_apply=%region_14.15 | all-reduce | flops 192 | bytes 1536 | tf_op jit(solution)/shard_map/psum | solution.py:24
  86.7 1.4 convolution_convert_fusion.1
  88.2 44.7 %all_to_all.25 = bf16[32,32,128]{2,1,0:T(8,128)(2,1)} all-to-all(bf16[32,32,128]{2,1,0:T(8,128)(2,1)S(1)} %bitcast.146), channel_id=1, replica_groups=mesh['sp'=32,'tp_0'=4,'tp_1'=4] {'sp'}, dimensions={0} | all-to-all | bytes 524288 | tf_op jit(solution)/shard_map/all_to_all | solution.py:122
  132.9 58.5 %all-gather.2.cloned.1.call-done = bf16[32,32,2048]{2,1,0:T(8,128)(2,1)} async-done(((bf16[32,32,128]{2,1,0:T(8,128)(2,1)}), bf16[32,32,2048]{2,1,0:T(8,128)(2,1)}) %all-gather.2.cloned.1.call-update) | async-done | bytes 4194320 | tf_op jit(solution)/shard_map/all_gather | solution.py:121
  191.4 4.8 %fusion.1 = f32[32,1,32,256]{3,2,0,1:T(8,128)} fusion(bf16[32,32,2048]{2,1,0:T(8,128)(2,1)} %all-gather.2.cloned.1.call-done, bf16[1,2048,256]{2,1,0:T(8,128)(2,1)} %param.25), kind=kOutput, calls=%fused_computation.8 | convolution fusion | flops 1074003968 | bytes 6291456 | tf_op jit(solution)/shard_map/sjcd,jdf->sjcf/dot_general | solution.py:132
  196.2 8.9 %convert_bitcast_fusion = bf16[1,32,4,16,8,128]{5,4,3,2,1,0:T(8,128)(2,1)} fusion(bf16[1,256,2048]{2,1,0:T(8,128)(2,1)S(1)} %copy-done, bf16[32,32,2048]{2,1,0:T(8,128)(2,1)} %all-gather.2.cloned.1.call-done, bf16[1,2048,256]{2,1,0:T(8,128)(2,1)S(1)} %copy-done.8, f32[32,1,32,256]{3,2,0,1:T(8,128)} %fusion.1), kind=kOutput, calls=%fused_computation.2 | convolution fusion | flops 2151940096 | bytes 11534336 | tf_op jit(solution)/shard_map/sjcf,jfd->sjcd/dot_general | solution.py:143
  205.1 3.3 %copy.39 = bf16[1,32,4,16,8,128]{5,4,2,1,0,3:T(8,128)(2,1)S(1)} copy(bf16[1,32,4,16,8,128]{5,4,3,2,1,0:T(8,128)(2,1)} %convert_bitcast_fusion) | data formatting | bytes 8388608 | tf_op jit(solution)/shard_map/reshape | solution.py:30
  208.4 54.5 %all_to_all.26 = bf16[16,32,1,32,128]{4,3,1,2,0:T(8,128)(2,1)} all-to-all(bf16[16,32,1,32,128]{4,3,1,2,0:T(8,128)(2,1)S(1)} %bitcast.143), channel_id=1, replica_groups=mesh['sp'=32,'tp_0'=4,'tp_1'=4] {'tp_0','tp_1'}, dimensions={0} | all-to-all | bytes 8388608 | tf_op jit(solution)/shard_map/all_to_all | solution.py:36
  262.8 3.5 %reduce_sum.86 = bf16[32,32,128]{2,1,0:T(8,128)(2,1)} reduce(bf16[16,32,1,32,128]{4,3,1,2,0:T(8,128)(2,1)} %all_to_all.26, bf16[]{:T(256)} %constant.38.clone.1), dimensions={0,2}, to_apply=%region_15.16 | reduce | flops 1966080 | bytes 4456450 | tf_op jit(solution)/shard_map/reduce_sum | solution.py:37
  266.4 15.5 %all-to-all-start.4 = ((bf16[32,32,128]{2,1,0:T(8,128)(2,1)}), bf16[32,32,128]{2,1,0:T(8,128)(2,1)S(1)}, u32[]{:S(2)}, u32[]{:S(2)}) async-start(bf16[32,32,128]{2,1,0:T(8,128)(2,1)} %reduce_sum.86), calls=%async_computation.4 | async-start | bytes 524288 | tf_op jit(solution)/shard_map/all_to_all | solution.py:147
  282.2 22.0 %all-to-all-done.4 = bf16[32,32,128]{2,1,0:T(8,128)(2,1)S(1)} async-done(((bf16[32,32,128]{2,1,0:T(8,128)(2,1)}), bf16[32,32,128]{2,1,0:T(8,128)(2,1)S(1)}, u32[]{:S(2)}, u32[]{:S(2)}) %all-to-all-start.4) | async-done | bytes 262176 | tf_op jit(solution)/shard_map/all_to_all | solution.py:147
  304.2 1.9 gather_fusion
  (51 shorter events, 9.6 us)
Async XLA Ops:
  6.5 189.7 %copy-start = (bf16[1,256,2048]{2,1,0:T(8,128)(2,1)S(1)}, bf16[1,256,2048]{2,1,0:T(8,128)(2,1)}, u32[]{:S(2)}) copy-start(bf16[1,256,2048]{2,1,0:T(8,128)(2,1)} %param.27) | copy-start | bytes 3145732
  6.5 31.9 %copy-start.6 = (s32[192,4]{0,1:T(4,128)S(1)}, s32[192,4]{0,1:T(4,128)}, u32[]{:S(2)}) copy-start(s32[192,4]{0,1:T(4,128)} %param.23) | copy-start | bytes 9220
  6.5 47.0 %copy-start.5 = (f32[2048]{0:T(1024)S(1)}, f32[2048]{0:T(1024)}, u32[]{:S(2)}) copy-start(f32[2048]{0:T(1024)} %param.20) | copy-start | bytes 24580
  7.5 8.8 %collective-permute-start = (bf16[30,128]{1,0:T(8,128)(2,1)S(1)}, bf16[30,128]{1,0:T(8,128)(2,1)S(1)}, u32[]{:S(2)}, u32[]{:S(2)}) collective-permute-start(bf16[30,128]{1,0:T(8,128)(2,1)S(1)} %slice.258), channel_id=1, source_target_pairs={{0,16},{16,32},{32,48},{48,64},{64,80},{80,96},{96,112},{112,128},... | collective-permute-start | bytes 23048 | tf_op jit(solution)/shard_map/ppermute | solution.py:19
  34.8 18.4 %all-to-all-start = ((bf16[16,12,2048]{2,1,0:T(8,128)(2,1)}), bf16[16,12,2048]{2,1,0:T(8,128)(2,1)S(1)}, u32[]{:S(2)}, u32[]{:S(2)}) async-start(bf16[16,12,2048]{2,1,0:T(8,128)(2,1)} %reshape.122), calls=%async_computation | async-start | bytes 2097152 | tf_op jit(solution)/shard_map/all_to_all | solution.py:36
  38.5 33.9 %copy-start.1 = (bf16[2048,128]{1,0:T(8,128)(2,1)S(1)}, bf16[2048,128]{1,0:T(8,128)(2,1)}, u32[]{:S(2)}) copy-start(bf16[2048,128]{1,0:T(8,128)(2,1)} %param.21) | copy-start | bytes 1572868
  38.5 33.9 %copy-start.2 = (bf16[192,128]{1,0:T(8,128)(2,1)S(1)}, bf16[192,128]{1,0:T(8,128)(2,1)}, u32[]{:S(2)}) copy-start(bf16[192,128]{1,0:T(8,128)(2,1)} %param.14) | copy-start | bytes 147460
  54.7 17.4 %all-to-all-start.1 = ((bf16[16,12,2048]{2,1,0:T(8,128)(2,1)}), bf16[16,12,2048]{2,1,0:T(8,128)(2,1)S(1)}, u32[]{:S(2)}, u32[]{:S(2)}) async-start(bf16[16,12,2048]{2,1,0:T(8,128)(2,1)} %broadcast_in_dim.2), calls=%async_computation.1 | async-start | bytes 2097152 | tf_op jit(solution)/shard_map/all_to_all | solution.py:42
  58.5 133.0 %all-gather.2.cloned.1.call-start = ((), (), s32[]{:S(2)}) async-start(), calls=%async_computation.5 | async-start | bytes 4456448 | tf_op jit(solution)/shard_map/all_gather | solution.py:121
  60.7 0.6 copy-start.3
  132.9 63.4 %copy-start.8 = (bf16[1,2048,256]{2,1,0:T(8,128)(2,1)S(1)}, bf16[1,2048,256]{2,1,0:T(8,128)(2,1)}, u32[]{:S(2)}) copy-start(bf16[1,2048,256]{2,1,0:T(8,128)(2,1)} %param.26) | copy-start | bytes 3145732
  262.8 19.2 %copy-start.7 = (f32[192,4]{0,1:T(4,128)S(1)}, f32[192,4]{0,1:T(4,128)}, u32[]{:S(2)}) copy-start(f32[192,4]{0,1:T(4,128)} %param.24) | copy-start | bytes 9220
  262.8 19.3 %copy-start.4 = (s32[768]{0:T(1024)S(1)}, s32[768]{0:T(1024)}, u32[]{:S(2)}) copy-start(s32[768]{0:T(1024)} %copy-done.3) | copy-start | bytes 9220
  266.4 37.8 %all-to-all-start.4 = ((bf16[32,32,128]{2,1,0:T(8,128)(2,1)}), bf16[32,32,128]{2,1,0:T(8,128)(2,1)S(1)}, u32[]{:S(2)}, u32[]{:S(2)}) async-start(bf16[32,32,128]{2,1,0:T(8,128)(2,1)} %reduce_sum.86), calls=%async_computation.4 | async-start | bytes 524288 | tf_op jit(solution)/shard_map/all_to_all | solution.py:147
Sparse Core Ops, SparseCore 0:
  133.0 58.3 all-gather.1
where the time goes:
time: 315 us; the launch traced here: 314 us
  blocking collectives  128 us (41%)
  waiting for transfers between devices  106 us (34%)
  starting transfers between devices  27.8 us (9%)
  matrix products  17 us (5%)
  between operations  13.7 us (4%)
  local copies, waits for them, and re-layouts  11.2 us (4%)
  other arithmetic  9.51 us (3%)
    all_gather x1, waiting for transfers between devices, shards(): lax.all_gather(lax.all_to_all(outgoing, 'sp', split_axis=0, concat_axis=0...  58.5 us
    all_to_all x1, blocking collectives, summed_on_arrival(): lax.all_to_all(pieces, axis, split_axis=0, concat_axis=0, tiled=True)  54.5 us
    all_to_all x1, blocking collectives, shards(): lax.all_to_all(outgoing, 'sp', split_axis=0, concat_axis=0, tiled=True)  44.7 us
    psum x4, blocking collectives, over_axes(): value = lax.psum(value, axis)  29.2 us
    all_to_all x1, waiting for transfers between devices, shards(): lax.all_to_all(summed.reshape(sources * local_experts, count, summed.shap...  22 us
    all_to_all x1, starting transfers between devices, shards(): lax.all_to_all(summed.reshape(sources * local_experts, count, summed.shap...  15.5 us
    all_to_all x1, waiting for transfers between devices, summed_on_arrival(): lax.all_to_all(pieces, axis, split_axis=0, concat_axis=0, tiled=True)  14.4 us
    all_to_all x1, waiting for transfers between devices, from_everyone(): return lax.all_to_all(copies, axis, split_axis=0, concat_axis=0, tiled=True)  9.49 us
  transfers between devices with their start and end apart: 5, of which 5 were waited for; matrix products, arithmetic and copies ran while one was open for 2% of the time, Pallas kernels for 0%

commit v1 on v0

--- a/solution.py
+++ b/solution.py
@@ -11,6 +11,13 @@
 epsilon = 1e-05
 clamp_limit = 7.0
 swish_slope = 1.702
+
+
+def all_by_exchange(x, axis, d):
+    size = lax.axis_size(axis)
+    pieces = jnp.stack([x for _ in range(size)])
+    pieces = lax.all_to_all(pieces, axis, split_axis=0, concat_axis=0)
+    return jnp.concatenate(pieces, axis=d)
 
 
 def from_behind(block, axis, distance):
@@ -118,11 +125,8 @@
         .astype(jnp.bfloat16)
         .reshape(E, CAP, feat_local)
     )
-    received = lax.all_gather(
-        lax.all_to_all(outgoing, "sp", split_axis=0, concat_axis=0, tiled=True),
-        TP,
-        axis=2,
-        tiled=True,
+    received = all_by_exchange(
+        lax.all_to_all(outgoing, "sp", split_axis=0, concat_axis=0, tiled=True), TP, 2
     )
     local_experts = gate_experts.shape[0]
     sources = received.shape[0] // local_experts

time: 315 us -> 286 us (0.908)
  waiting for transfers between devices: 106 us -> 47.7 us
  blocking collectives: 128 us -> 180 us
  between operations: 13.7 us -> 0.27 us
  starting transfers between devices: 27.8 us -> 19.5 us
    all_gather x1 -> x0, waiting for transfers between devices: 58.5 us -> none  [shards(): lax.all_gather(lax.all_to_all(outgoing, 'sp', split_axis=0, concat_axis=0...]
    all_to_all x0 -> x1, blocking collectives: none -> 52.8 us  [all_by_exchange(): pieces = lax.all_to_all(pieces, axis, split_axis=0, concat_axis=0)]
    all_to_all x1, starting transfers between devices: 15.5 us -> 7.24 us  [shards(): lax.all_to_all(summed.reshape(sources * local_experts, count, summed.shap...]
  transfers between devices with their start and end apart: 5 -> 4, of which waited for: 5 -> 4; matrix products, arithmetic and copies ran while one was open for 2% -> 2% of each run, Pallas kernels for 0% -> 0%
where the time goes in v1:
time: 286 us; the launch traced here: 285 us
  blocking collectives  180 us (63%)
  waiting for transfers between devices  47.7 us (17%)
  starting transfers between devices  19.5 us (7%)
  matrix products  14.8 us (5%)
  local copies, waits for them, and re-layouts  13.9 us (5%)
  other arithmetic  9.51 us (3%)
    all_to_all x1, blocking collectives, summed_on_arrival(): lax.all_to_all(pieces, axis, split_axis=0, concat_axis=0, tiled=True)  53.1 us
    all_to_all x1, blocking collectives, all_by_exchange(): pieces = lax.all_to_all(pieces, axis, split_axis=0, concat_axis=0)  52.8 us
    all_to_all x1, blocking collectives, shards(): lax.all_to_all(outgoing, 'sp', split_axis=0, concat_axis=0, tiled=True)  44.6 us
    psum x4, blocking collectives, over_axes(): value = lax.psum(value, axis)  29.2 us
    all_to_all x1, waiting for transfers between devices, shards(): lax.all_to_all(summed.reshape(sources * local_experts, count, summed.shap...  22 us
    all_to_all x1, waiting for transfers between devices, summed_on_arrival(): lax.all_to_all(pieces, axis, split_axis=0, concat_axis=0, tiled=True)  14.4 us
    all_to_all x1, waiting for transfers between devices, from_everyone(): return lax.all_to_all(copies, axis, split_axis=0, concat_axis=0, tiled=True)  9.53 us
    dot_general x1, matrix products, shards(): jnp.einsum('sjcf,jfd->sjcd', hidden, down_experts, preferred_element_type...  9.12 us
  transfers between devices with their start and end apart: 4, of which 4 were waited for; matrix products, arithmetic and copies ran while one was open for 2% of the time, Pallas kernels for 0%

profile of v1, /device:TPU:1, one launch (start us, length us, event | category | flops | bytes accessed | tf_op | source)
XLA Modules:
  0.0 285.5 jit_solution(10509144264090167878)
XLA Ops:
  1.0 4.9 %collective-permute-start = (bf16[30,128]{1,0:T(8,128)(2,1)S(1)}, bf16[30,128]{1,0:T(8,128)(2,1)S(1)}, u32[]{:S(2)}, u32[]{:S(2)}) collective-permute-start(bf16[30,128]{1,0:T(8,128)(2,1)S(1)} %slice.258), channel_id=1, source_target_pairs={{0,16},{16,32},{32,48},{48,64},{64,80},{80,96},{96,112},{112,128},... | collective-permute-start | bytes 23048 | tf_op jit(solution)/shard_map/ppermute | solution.py:26
  7.9 1.9 collective-permute-done
  10.3 7.1 %all-reduce.1 = (f32[192]{0:T(256)S(1)}, f32[192]{0:T(256)S(1)}) all-reduce(f32[192]{0:T(256)S(1)} %get-tuple-element.6, f32[192]{0:T(256)S(1)} %get-tuple-element.5), channel_id=1, replica_groups=mesh['sp'=32,'tp_0'=4,'tp_1'=4] {'tp_0'}, use_global_device_ids=true, to_apply=%region_4.0 | all-reduce | flops 384 | bytes 3072 | tf_op jit(solution)/shard_map/psum | solution.py:31
  17.4 8.2 %all-reduce = (f32[192]{0:T(256)S(1)}, f32[192]{0:T(256)S(1)}) all-reduce(f32[192]{0:T(256)S(1)} %get-tuple-element.9, f32[192]{0:T(256)S(1)} %get-tuple-element.10), channel_id=1, replica_groups=mesh['sp'=32,'tp_0'=4,'tp_1'=4] {'tp_1'}, use_global_device_ids=true, to_apply=%region_5.0 | all-reduce | flops 384 | bytes 3072 | tf_op jit(solution)/shard_map/psum | solution.py:31
  25.6 1.5 convolution_convert_fusion
  28.3 3.7 %all-to-all-start = ((bf16[16,12,2048]{2,1,0:T(8,128)(2,1)}), bf16[16,12,2048]{2,1,0:T(8,128)(2,1)S(1)}, u32[]{:S(2)}, u32[]{:S(2)}) async-start(bf16[16,12,2048]{2,1,0:T(8,128)(2,1)} %reshape.128), calls=%async_computation | async-start | bytes 2097152 | tf_op jit(solution)/shard_map/all_to_all | solution.py:43
  32.3 14.4 %all-to-all-done = bf16[16,12,2048]{2,1,0:T(8,128)(2,1)S(1)} async-done(((bf16[16,12,2048]{2,1,0:T(8,128)(2,1)}), bf16[16,12,2048]{2,1,0:T(8,128)(2,1)S(1)}, u32[]{:S(2)}, u32[]{:S(2)}) %all-to-all-start) | async-done | bytes 786464 | tf_op jit(solution)/shard_map/all_to_all | solution.py:43
  48.2 3.7 %all-to-all-start.1 = ((bf16[16,12,2048]{2,1,0:T(8,128)(2,1)}), bf16[16,12,2048]{2,1,0:T(8,128)(2,1)S(1)}, u32[]{:S(2)}, u32[]{:S(2)}) async-start(bf16[16,12,2048]{2,1,0:T(8,128)(2,1)} %broadcast_in_dim.2), calls=%async_computation.1 | async-start | bytes 2097152 | tf_op jit(solution)/shard_map/all_to_all | solution.py:49
  51.9 1.7 reduce-window.6
  56.1 9.5 %all-to-all-done.1 = bf16[16,12,2048]{2,1,0:T(8,128)(2,1)S(1)} async-done(((bf16[16,12,2048]{2,1,0:T(8,128)(2,1)}), bf16[16,12,2048]{2,1,0:T(8,128)(2,1)S(1)}, u32[]{:S(2)}, u32[]{:S(2)}) %all-to-all-start.1) | async-done | bytes 786464 | tf_op jit(solution)/shard_map/all_to_all | solution.py:49
  66.3 7.2 %psum.46 = f32[192]{0:T(256)S(1)} all-reduce(f32[192]{0:T(256)S(1)} %get-tuple-element.47), channel_id=1, replica_groups=mesh['sp'=32,'tp_0'=4,'tp_1'=4] {'tp_0'}, use_global_device_ids=true, to_apply=%region_13.14 | all-reduce | flops 192 | bytes 1536 | tf_op jit(solution)/shard_map/psum | solution.py:31
  73.6 6.6 %psum.47 = f32[192]{0:T(256)S(1)} all-reduce(f32[192]{0:T(256)S(1)} %psum.46), channel_id=1, replica_groups=mesh['sp'=32,'tp_0'=4,'tp_1'=4] {'tp_1'}, use_global_device_ids=true, to_apply=%region_14.15 | all-reduce | flops 192 | bytes 1536 | tf_op jit(solution)/shard_map/psum | solution.py:31
  80.2 1.4 convolution_convert_fusion.1
  81.7 44.6 %all_to_all.30 = bf16[32,32,128]{2,1,0:T(8,128)(2,1)S(1)} all-to-all(bf16[32,32,128]{2,1,0:T(8,128)(2,1)S(1)} %bitcast.176), channel_id=1, replica_groups=mesh['sp'=32,'tp_0'=4,'tp_1'=4] {'sp'}, dimensions={0} | all-to-all | bytes 524288 | tf_op jit(solution)/shard_map/all_to_all | solution.py:129
  127.0 52.8 %all_to_all.31 = bf16[16,32,32,128]{3,2,1,0:T(8,128)(2,1)S(1)} all-to-all(bf16[16,32,32,128]{3,2,1,0:T(8,128)(2,1)S(1)} %stack.2), channel_id=1, replica_groups=mesh['sp'=32,'tp_0'=4,'tp_1'=4] {'tp_0','tp_1'}, dimensions={0} | all-to-all | bytes 8388608 | tf_op jit(solution)/shard_map/all_to_all | solution.py:19
  179.8 1.9 copy-done.1
  181.7 2.3 fusion.10
  184.1 9.1 %convert_bitcast_fusion = bf16[1,32,4,16,8,128]{5,4,3,2,1,0:T(8,128)(2,1)} fusion(bf16[1,256,2048]{2,1,0:T(8,128)(2,1)S(1)} %copy-done, bf16[1,2048,256]{2,1,0:T(8,128)(2,1)} %param.26, f32[32,1,32,256]{3,2,0,1:T(8,128)} %fusion.10, bf16[16,32,32,128]{3,2,1,0:T(8,128)(2,1)} %copy-done.1), kind=kOutput, calls=%fused_computation.6 | convolution fusion | flops 2151940096 | bytes 11534336 | tf_op jit(solution)/shard_map/sjcf,jfd->sjcd/dot_general | solution.py:147
  193.2 3.3 %copy.68 = bf16[1,32,4,16,8,128]{5,4,2,1,0,3:T(8,128)(2,1)S(1)} copy(bf16[1,32,4,16,8,128]{5,4,3,2,1,0:T(8,128)(2,1)} %convert_bitcast_fusion) | data formatting | bytes 8388608 | tf_op jit(solution)/shard_map/reshape | solution.py:37
  196.5 53.1 %all_to_all.32 = bf16[16,32,1,32,128]{4,3,1,2,0:T(8,128)(2,1)} all-to-all(bf16[16,32,1,32,128]{4,3,1,2,0:T(8,128)(2,1)S(1)} %bitcast.173), channel_id=1, replica_groups=mesh['sp'=32,'tp_0'=4,'tp_1'=4] {'tp_0','tp_1'}, dimensions={0} | all-to-all | bytes 8388608 | tf_op jit(solution)/shard_map/all_to_all | solution.py:43
  249.6 3.5 %reduce_sum.86 = bf16[32,32,128]{2,1,0:T(8,128)(2,1)} reduce(bf16[16,32,1,32,128]{4,3,1,2,0:T(8,128)(2,1)} %all_to_all.32, bf16[]{:T(256)} %constant.38.clone.1), dimensions={0,2}, to_apply=%region_15.16 | reduce | flops 1966080 | bytes 4456450 | tf_op jit(solution)/shard_map/reduce_sum | solution.py:44
  253.1 7.2 %all-to-all-start.5 = ((bf16[32,32,128]{2,1,0:T(8,128)(2,1)}), bf16[32,32,128]{2,1,0:T(8,128)(2,1)S(1)}, u32[]{:S(2)}, u32[]{:S(2)}) async-start(bf16[32,32,128]{2,1,0:T(8,128)(2,1)} %reduce_sum.86), calls=%async_computation.5 | async-start | bytes 524288 | tf_op jit(solution)/shard_map/all_to_all | solution.py:151
  260.7 22.0 %all-to-all-done.5 = bf16[32,32,128]{2,1,0:T(8,128)(2,1)S(1)} async-done(((bf16[32,32,128]{2,1,0:T(8,128)(2,1)}), bf16[32,32,128]{2,1,0:T(8,128)(2,1)S(1)}, u32[]{:S(2)}, u32[]{:S(2)}) %all-to-all-start.5) | async-done | bytes 262176 | tf_op jit(solution)/shard_map/all_to_all | solution.py:151
  282.6 1.9 gather_fusion
  (52 shorter events, 11.5 us)
Async XLA Ops:
  0.0 184.1 %copy-start = (bf16[1,256,2048]{2,1,0:T(8,128)(2,1)S(1)}, bf16[1,256,2048]{2,1,0:T(8,128)(2,1)}, u32[]{:S(2)}) copy-start(bf16[1,256,2048]{2,1,0:T(8,128)(2,1)} %param.27) | copy-start | bytes 3145732
  0.0 31.9 %copy-start.7 = (s32[192,4]{0,1:T(4,128)S(1)}, s32[192,4]{0,1:T(4,128)}, u32[]{:S(2)}) copy-start(s32[192,4]{0,1:T(4,128)} %param.23) | copy-start | bytes 9220
  0.0 47.0 %copy-start.6 = (f32[2048]{0:T(1024)S(1)}, f32[2048]{0:T(1024)}, u32[]{:S(2)}) copy-start(f32[2048]{0:T(1024)} %param.20) | copy-start | bytes 24580
  1.0 8.8 %collective-permute-start = (bf16[30,128]{1,0:T(8,128)(2,1)S(1)}, bf16[30,128]{1,0:T(8,128)(2,1)S(1)}, u32[]{:S(2)}, u32[]{:S(2)}) collective-permute-start(bf16[30,128]{1,0:T(8,128)(2,1)S(1)} %slice.258), channel_id=1, source_target_pairs={{0,16},{16,32},{32,48},{48,64},{64,80},{80,96},{96,112},{112,128},... | collective-permute-start | bytes 23048 | tf_op jit(solution)/shard_map/ppermute | solution.py:26
  28.3 18.4 %all-to-all-start = ((bf16[16,12,2048]{2,1,0:T(8,128)(2,1)}), bf16[16,12,2048]{2,1,0:T(8,128)(2,1)S(1)}, u32[]{:S(2)}, u32[]{:S(2)}) async-start(bf16[16,12,2048]{2,1,0:T(8,128)(2,1)} %reshape.128), calls=%async_computation | async-start | bytes 2097152 | tf_op jit(solution)/shard_map/all_to_all | solution.py:43
  31.9 33.9 %copy-start.2 = (bf16[2048,128]{1,0:T(8,128)(2,1)S(1)}, bf16[2048,128]{1,0:T(8,128)(2,1)}, u32[]{:S(2)}) copy-start(bf16[2048,128]{1,0:T(8,128)(2,1)} %param.21) | copy-start | bytes 1572868
  32.0 33.9 %copy-start.3 = (bf16[192,128]{1,0:T(8,128)(2,1)S(1)}, bf16[192,128]{1,0:T(8,128)(2,1)}, u32[]{:S(2)}) copy-start(bf16[192,128]{1,0:T(8,128)(2,1)} %param.14) | copy-start | bytes 147460
  48.2 17.4 %all-to-all-start.1 = ((bf16[16,12,2048]{2,1,0:T(8,128)(2,1)}), bf16[16,12,2048]{2,1,0:T(8,128)(2,1)S(1)}, u32[]{:S(2)}, u32[]{:S(2)}) async-start(bf16[16,12,2048]{2,1,0:T(8,128)(2,1)} %broadcast_in_dim.2), calls=%async_computation.1 | async-start | bytes 2097152 | tf_op jit(solution)/shard_map/all_to_all | solution.py:49
  54.1 0.6 copy-start.4
  127.0 54.7 %copy-start.9 = (bf16[1,2048,256]{2,1,0:T(8,128)(2,1)S(1)}, bf16[1,2048,256]{2,1,0:T(8,128)(2,1)}, u32[]{:S(2)}) copy-start(bf16[1,2048,256]{2,1,0:T(8,128)(2,1)} %param.25) | copy-start | bytes 3145732
  179.8 1.9 copy-start.1
  249.6 10.9 %copy-start.8 = (f32[192,4]{0,1:T(4,128)S(1)}, f32[192,4]{0,1:T(4,128)}, u32[]{:S(2)}) copy-start(f32[192,4]{0,1:T(4,128)} %param.24) | copy-start | bytes 9220
  249.6 11.0 %copy-start.5 = (s32[768]{0:T(1024)S(1)}, s32[768]{0:T(1024)}, u32[]{:S(2)}) copy-start(s32[768]{0:T(1024)} %copy-done.4) | copy-start | bytes 9220
  253.1 29.5 %all-to-all-start.5 = ((bf16[32,32,128]{2,1,0:T(8,128)(2,1)}), bf16[32,32,128]{2,1,0:T(8,128)(2,1)S(1)}, u32[]{:S(2)}, u32[]{:S(2)}) async-start(bf16[32,32,128]{2,1,0:T(8,128)(2,1)} %reduce_sum.86), calls=%async_computation.5 | async-start | bytes 524288 | tf_op jit(solution)/shard_map/all_to_all | solution.py:151
